TPU v7x, 32 devices: a whole 2x2x4 slice. The times are simulated.
32 devices in a mesh: ep: 8 (over z, x), tp: 4 (over y, core).
Axes of the slice: x: 2, y: 2, z: 4, core: 2. Of those that a mesh axis runs over, the one named last changes fastest.
Arguments:
- conv_value: bfloat16 [8192, 1024], P('ep', 'tp'), may hold values from -600 to 600
- conv_gate: bfloat16 [8192, 1024], P('ep', 'tp'), may hold values from -8 to 8
- depth_weight: float32 [31, 1024], replicated, may hold values from -1 to 1
- norm_gain: float32 [1024], replicated, may hold values from 0.1 to 1.9
- norm_shift: float32 [1024], replicated, may hold values from -3 to 3
- conv_out_weight: bfloat16 [1024, 2048], P('tp'), may hold values from -0.1875 to 0.1875
- moe_input: bfloat16 [12288, 2048], P(('ep', 'tp')), may hold values from -6 to 6
- moe_gain: float32 [2048], replicated, may hold values from 0.1 to 1.9
- route_experts: int32 [12288, 2], P(('ep', 'tp')), may hold values from 0 to 7, as said below
- route_scores: float32 [12288, 2], P(('ep', 'tp')), may hold values from -8 to 8
- expert_gate: bfloat16 [8, 2048, 512], P('ep'), may hold values from -0.125 to 0.125
- expert_up: bfloat16 [8, 2048, 512], P('ep'), may hold values from -0.125 to 0.125
- expert_down: bfloat16 [8, 512, 2048], P('ep'), may hold values from -1 to 1
Outputs:
- conv_out: bfloat16 [8192, 2048], P(('ep', 'tp'))
- moe_out: bfloat16 [12288, 2048], P(('ep', 'tp'))
Inputs may be any that keep to these rules, and one draw needn't show every extreme that they name: `route_experts`: each row names two different experts that lie in one group of 2 consecutive experts.
All inputs are finite; a program needn't handle non-finite values.
Results may differ from a plain program's by a relative error of at most 0.009.
Values may be sent and summed in bfloat16 or wider, within the bound.
A program may use at most 128 MiB of HBM per device.

v0:
```python
import jax
import jax.numpy as jnp
from jax import lax
from jax.sharding import PartitionSpec as P

CONV = 1024
TOP = 2


def passed_along(x, axis, by):
    peers = lax.axis_size(axis)
    pairs = [(i, i + by) for i in range(peers) if 0 <= i + by < peers]
    return lax.ppermute(x, axis, pairs)


def conv_half(conv_value, conv_gate, depth_weight, norm_gain, norm_shift, conv_out_weight):
    channels = conv_value.shape[1]
    length = conv_value.shape[0]
    first_col = lax.axis_index("tp") * channels
    taps = lax.dynamic_slice_in_dim(depth_weight, first_col, channels, 1)
    gains = lax.dynamic_slice_in_dim(norm_gain, first_col, channels, 0)
    shifts = lax.dynamic_slice_in_dim(norm_shift, first_col, channels, 0)
    gated = (conv_value.astype(jnp.float32) * jax.nn.sigmoid(conv_gate.astype(jnp.float32))).astype(
        jnp.bfloat16
    )
    reach = taps.shape[0] - 1
    earlier = passed_along(gated[length - reach :], "ep", 1)
    padded = jnp.concatenate([earlier, gated], 0).astype(jnp.float32)
    filtered = taps[0] * padded[0:length]
    for offset in range(1, reach + 1):
        filtered = filtered + taps[offset] * padded[offset : offset + length]
    sums, squares = lax.psum(
        (jnp.sum(filtered, axis=1), jnp.sum(filtered * filtered, axis=1)), "tp"
    )
    center = (sums / CONV)[:, None]
    spread = (squares / CONV)[:, None] - center * center
    normed = (filtered - center) * lax.rsqrt(spread + 1e-05) * gains + shifts
    activated = jax.nn.silu(normed).astype(jnp.bfloat16)
    partial_value = jnp.dot(activated, conv_out_weight, preferred_element_type=jnp.float32)
    return lax.psum_scatter(
        partial_value.astype(jnp.bfloat16).astype(jnp.float32).astype(jnp.bfloat16),
        "tp",
        scatter_dimension=0,
        tiled=True,
    )


def moe_half(moe_input, moe_gain, route_experts, route_scores, expert_gate, expert_up, expert_down):
    rows = moe_input.shape[0]
    model_width = moe_input.shape[1]
    experts_all = lax.axis_size("ep")
    capacity = 2 * (3 * TOP * rows // (4 * experts_all))
    widened = moe_input.astype(jnp.float32)
    normal_in = (
        widened * lax.rsqrt(jnp.mean(widened * widened, axis=-1, keepdims=True) + 1e-06) * moe_gain
    ).astype(jnp.bfloat16)
    chosen = route_experts.reshape(-1)
    onehot = (chosen[:, None] == jnp.arange(experts_all, dtype=jnp.int32)[None, :]).astype(
        jnp.int32
    )
    slot_rank = jnp.sum(jnp.cumsum(onehot, axis=0) * onehot, axis=-1) - 1
    slot_index = jnp.where(
        slot_rank < capacity, chosen * capacity + slot_rank, experts_all * capacity
    )
    source_row = jnp.arange(rows * TOP, dtype=jnp.int32) // TOP
    slot_token = (
        jnp.full((experts_all * capacity,), rows, jnp.int32)
        .at[slot_index]
        .set(source_row, mode="drop")
    )
    padded_in = jnp.concatenate([normal_in, jnp.zeros((1, model_width), jnp.bfloat16)], 0)
    send_buffer = padded_in[slot_token].reshape(experts_all, capacity, model_width)
    arrived = lax.all_to_all(send_buffer, "ep", split_axis=0, concat_axis=0, tiled=True)
    flat_rows = arrived.reshape(-1, model_width)
    gate_act = jnp.dot(flat_rows, expert_gate[0], preferred_element_type=jnp.float32)
    up_act = jnp.dot(flat_rows, expert_up[0], preferred_element_type=jnp.float32)
    inner = (jax.nn.silu(gate_act) * up_act).astype(jnp.bfloat16)
    result = jnp.dot(inner, expert_down[0], preferred_element_type=jnp.float32).astype(jnp.bfloat16)
    returned = lax.all_to_all(
        result.reshape(arrived.shape), "ep", split_axis=0, concat_axis=0, tiled=True
    )
    returned_flat = jnp.concatenate(
        [
            returned.reshape(experts_all * capacity, model_width),
            jnp.zeros((1, model_width), jnp.bfloat16),
        ],
        0,
    )
    picked = returned_flat[slot_index].reshape(rows, TOP, model_width)
    group_gate = jax.nn.sigmoid(route_scores[:, 0])
    first_weight = (group_gate * jax.nn.sigmoid(route_scores[:, 1]))[:, None]
    second_weight = (group_gate * jax.nn.sigmoid(-route_scores[:, 1]))[:, None]
    combined = first_weight * picked[:, 0].astype(jnp.float32) + second_weight * picked[
        :, 1
    ].astype(jnp.float32)
    return combined.astype(jnp.bfloat16)


def on_device(
    conv_value,
    conv_gate,
    depth_weight,
    norm_gain,
    norm_shift,
    conv_out_weight,
    moe_input,
    moe_gain,
    route_experts,
    route_scores,
    expert_gate,
    expert_up,
    expert_down,
):
    conv_out = conv_half(
        conv_value, conv_gate, depth_weight, norm_gain, norm_shift, conv_out_weight
    )
    moe_out = moe_half(
        moe_input, moe_gain, route_experts, route_scores, expert_gate, expert_up, expert_down
    )
    return (conv_out, moe_out)


def solution(mesh):
    in_specs = (
        P("ep", "tp"),
        P("ep", "tp"),
        P(),
        P(),
        P(),
        P("tp", None),
        P(("ep", "tp"), None),
        P(),
        P(("ep", "tp"), None),
        P(("ep", "tp"), None),
        P("ep", None, None),
        P("ep", None, None),
        P("ep", None, None),
    )
    out_specs = (P(("ep", "tp"), None), P(("ep", "tp"), None))
    return jax.shard_map(
        on_device, mesh=mesh, in_specs=in_specs, out_specs=out_specs, check_vma=False
    )
```

profile of v0, /device:TPU:0, one launch (start us, length us, event | category | flops | bytes accessed | tf_op | source)
XLA Modules:
  0.0 313.0 jit_solution(3297898859941585447)
XLA Ops:
  9.1 1.7 reduce-window.6
  11.8 3.4 %scatter_custom_fusion = s32[1152]{0:T(1024)S(1)} fusion(s32[768]{0:T(1024)S(1)} %get-tuple-element.7, s32[768]{0:T(1024)S(1)} %add_select_fusion, s32[]{:T(128)} %constant.59.clone.1), kind=kCustom, calls=%fused_computation.109 | custom fusion | bytes 4612 | tf_op jit(solution)/shard_map/scatter | solution.py:69
  15.2 1.8 fusion
  17.0 1.8 fusion.2
  18.8 1.3 concatenate.10
  20.1 12.3 %gather_fusion = bf16[1152,2048]{1,0:T(8,128)(2,1)} fusion(bf16[385,2048]{1,0:T(8,128)(2,1)} %concatenate.10, s32[2048]{0:T(1024)S(1)} %pad_clamp_fusion), kind=kCustom, calls=%fused_computation | custom fusion | bytes 9441792 | tf_op jit(solution)/shard_map/gather | solution.py:72
  32.4 7.4 %all-to-all-start = ((bf16[8,144,2048]{2,1,0:T(8,128)(2,1)}), bf16[8,144,2048]{2,1,0:T(8,128)(2,1)}, u32[]{:S(2)}, u32[]{:S(2)}) async-start(bf16[8,144,2048]{2,1,0:T(8,128)(2,1)} %bitcast.67), calls=%async_computation.1 | async-start | bytes 9437184 | tf_op jit(solution)/shard_map/all_to_all | solution.py:73
  40.9 4.1 %collective-permute-start = (bf16[30,256]{1,0:T(8,128)(2,1)S(1)}, bf16[30,256]{1,0:T(8,128)(2,1)S(1)}, u32[]{:S(2)}, u32[]{:S(2)}) collective-permute-start(bf16[30,256]{1,0:T(8,128)(2,1)S(1)} %slice.281), channel_id=1, source_target_pairs={{0,4},{4,8},{8,12},{12,16},{16,20},{20,24},{24,28},{1,5},{5,9},{9,... | collective-permute-start | bytes 46088 | tf_op jit(solution)/shard_map/ppermute | solution.py:13
  45.0 1.4 constant_dynamic-slice_fusion
  46.4 1.2 fusion.63
  49.2 29.1 %collective-permute-done = bf16[30,256]{1,0:T(8,128)(2,1)S(1)} collective-permute-done((bf16[30,256]{1,0:T(8,128)(2,1)S(1)}, bf16[30,256]{1,0:T(8,128)(2,1)S(1)}, u32[]{:S(2)}, u32[]{:S(2)}) %collective-permute-start) | collective-permute-done | bytes 15392 | tf_op jit(solution)/shard_map/ppermute | solution.py:13
  79.4 64.9 %all-to-all-done = bf16[8,144,2048]{2,1,0:T(8,128)(2,1)} async-done(((bf16[8,144,2048]{2,1,0:T(8,128)(2,1)}), bf16[8,144,2048]{2,1,0:T(8,128)(2,1)}, u32[]{:S(2)}, u32[]{:S(2)}) %all-to-all-start) | async-done | bytes 4718624 | tf_op jit(solution)/shard_map/all_to_all | solution.py:73
  144.3 7.0 %fusion.8 = f32[1152,512]{1,0:T(8,128)} fusion(bf16[1152,2048]{1,0:T(8,128)(2,1)} %bitcast.35, bf16[1,2048,512]{2,1,0:T(8,128)(2,1)} %param.23), kind=kOutput, calls=%fused_computation.18 | convolution fusion | flops 2415919104 | bytes 9175040 | tf_op jit(solution)/shard_map/dot_general | solution.py:75
  151.4 11.0 %convolution_convert_fusion = bf16[1152,2048]{1,0:T(8,128)(2,1)} fusion(bf16[1,512,2048]{2,1,0:T(8,128)(2,1)S(1)} %copy-done, bf16[1152,2048]{1,0:T(8,128)(2,1)} %bitcast.35, f32[1152,512]{1,0:T(8,128)} %fusion.8, bf16[1,2048,512]{2,1,0:T(8,128)(2,1)} %param.24), kind=kOutput, calls=%fused_computation.3 | convolution fusion | flops 4837736448 | bytes 15990784 | tf_op jit(solution)/shard_map/dot_general | solution.py:78
  162.4 4.6 %all-to-all-start.1 = ((bf16[8,144,2048]{2,1,0:T(8,128)(2,1)}), bf16[8,144,2048]{2,1,0:T(8,128)(2,1)}, u32[]{:S(2)}, u32[]{:S(2)}) async-start(bf16[8,144,2048]{2,1,0:T(8,128)(2,1)} %bitcast.68), calls=%async_computation.2 | async-start | bytes 9437184 | tf_op jit(solution)/shard_map/all_to_all | solution.py:79
  167.0 5.1 %fusion.60 = (f32[1024]{0:T(1024)S(1)}, f32[1024]{0:T(1024)S(1)}, f32[1024,256]{1,0:T(8,128)}) fusion(f32[1054,256]{1,0:T(8,128)S(1)} %maximum_convert_fusion, f32[256]{0:T(256)S(1)} %bitcast.101, f32[256]{0:T(256)S(1)} %bitcast.72, f32[256]{0:T(256)S(1)} %bitcast.73, f32[256]{0:T(256)S(1)} %bitcast.74, f32[256]{0:T(256)S(1)} %bitcast.75, ...), kind=kLoop, calls=%fused_computation.127 | loop fusion | flops 16775168 | bytes 33594368 | tf_op jit(solution)/shard_map/reduce_sum | solution.py:33
  172.1 6.7 %all-reduce.2 = (f32[1024]{0:T(1024)S(1)}, f32[1024]{0:T(1024)S(1)}) all-reduce(f32[1024]{0:T(1024)S(1)} %get-tuple-element.3, f32[1024]{0:T(1024)S(1)} %get-tuple-element.2), channel_id=1, replica_groups=mesh['ep'=8,'tp'=4] {'tp'}, use_global_device_ids=true, to_apply=%region_3.0 | all-reduce | flops 2048 | bytes 16384 | tf_op jit(solution)/shard_map/psum | solution.py:32
  178.9 5.0 %convolution_convert_fusion.1 = bf16[1024,2048]{1,0:T(8,128)(2,1)} fusion(bf16[256,2048]{1,0:T(8,128)(2,1)} %param.18, f32[1024,256]{1,0:T(8,128)} %get-tuple-element.10, f32[256]{0:T(256)S(1)} %dynamic_slice.11, f32[256]{0:T(256)S(1)} %dynamic_slice.10, f32[1024]{0:T(1024)S(1)} %get-tuple-element.45, f32[1024]{0:T(1024)S(1)} %get-tuple-element.44), kind=kOutput, calls=%fused_computation.6 | convolution fusion | flops 1078198272 | bytes 6301696 | tf_op jit(solution)/shard_map/dot_general | solution.py:39
  184.7 87.7 %all-to-all-done.1 = bf16[8,144,2048]{2,1,0:T(8,128)(2,1)} async-done(((bf16[8,144,2048]{2,1,0:T(8,128)(2,1)}), bf16[8,144,2048]{2,1,0:T(8,128)(2,1)}, u32[]{:S(2)}, u32[]{:S(2)}) %all-to-all-start.1) | async-done | bytes 4718624 | tf_op jit(solution)/shard_map/all_to_all | solution.py:79
  272.4 5.2 %concatenate.11 = bf16[1153,2048]{1,0:T(8,128)(2,1)} pad(bf16[1152,2048]{1,0:T(8,128)(2,1)} %bitcast.40, bf16[]{:T(256)} %constant.58.clone.1), padding=0_1x0_0 | pad | bytes 9441282 | tf_op jit(solution)/shard_map/concatenate | solution.py:82
  277.6 10.0 %gather_fusion.1 = bf16[768,2048]{1,0:T(8,128)(2,1)} fusion(bf16[1153,2048]{1,0:T(8,128)(2,1)} %concatenate.11, s32[1024]{0:T(1024)S(1)} %pad_clamp_fusion.1), kind=kCustom, calls=%fused_computation.1 | custom fusion | bytes 6294528 | tf_op jit(solution)/shard_map/gather | solution.py:89
  287.6 6.0 %reshape.116 = bf16[384,2,2048]{2,1,0:T(2,128)(2,1)} reshape(bf16[768,2048]{1,0:T(8,128)(2,1)} %gather_fusion.1) | data formatting | bytes 6291456 | tf_op jit(solution)/shard_map/reshape | solution.py:89
  293.6 7.7 %fusion.62 = (bf16[384,1,2048]{2,1,0:T(2,128)(2,1)S(1)}, bf16[384,1,2048]{2,1,0:T(2,128)(2,1)S(1)}) fusion(bf16[384,2,2048]{2,1,0:T(2,128)(2,1)} %reshape.116), kind=kLoop, calls=%fused_computation.128 | loop fusion | bytes 6291456 | tf_op jit(solution)/shard_map/slice | solution.py:93
  301.3 4.9 %fusion.4 = bf16[384,2048]{1,0:T(8,128)(2,1)} fusion(bf16[384,1,2048]{2,1,0:T(2,128)(2,1)S(1)} %get-tuple-element.12, bf16[384,1,2048]{2,1,0:T(2,128)(2,1)S(1)} %get-tuple-element.11, f32[384]{0:T(512)S(1)} %get-tuple-element.5, f32[384]{0:T(512)S(1)} %get-tuple-element.4), kind=kLoop, calls=%fused_computation.13 | loop fusion | flops 4718592 | bytes 4721664 | tf_op jit(solution)/shard_map/convert_element_type | solution.py:96
  (39 shorter events, 7.4 us)
Async XLA Ops:
  7.2 144.2 %copy-start = (bf16[1,512,2048]{2,1,0:T(8,128)(2,1)S(1)}, bf16[1,512,2048]{2,1,0:T(8,128)(2,1)}, u32[]{:S(2)}) copy-start(bf16[1,512,2048]{2,1,0:T(8,128)(2,1)} %param.25) | copy-start | bytes 6291460
  32.4 7.4 %copy-start.2 = (bf16[1024,256]{1,0:T(8,128)(2,1)S(1)}, bf16[1024,256]{1,0:T(8,128)(2,1)}, u32[]{:S(2)}) copy-start(bf16[1024,256]{1,0:T(8,128)(2,1)} %param.14) | copy-start | bytes 1572868
  32.4 7.4 %copy-start.3 = (bf16[1024,256]{1,0:T(8,128)(2,1)S(1)}, bf16[1024,256]{1,0:T(8,128)(2,1)}, u32[]{:S(2)}) copy-start(bf16[1024,256]{1,0:T(8,128)(2,1)} %param.13) | copy-start | bytes 1572868
  32.4 111.9 %all-to-all-start = ((bf16[8,144,2048]{2,1,0:T(8,128)(2,1)}), bf16[8,144,2048]{2,1,0:T(8,128)(2,1)}, u32[]{:S(2)}, u32[]{:S(2)}) async-start(bf16[8,144,2048]{2,1,0:T(8,128)(2,1)} %bitcast.67), calls=%async_computation.1 | async-start | bytes 9437184 | tf_op jit(solution)/shard_map/all_to_all | solution.py:73
  40.1 0.8 copy-start.1
  40.9 37.3 %collective-permute-start = (bf16[30,256]{1,0:T(8,128)(2,1)S(1)}, bf16[30,256]{1,0:T(8,128)(2,1)S(1)}, u32[]{:S(2)}, u32[]{:S(2)}) collective-permute-start(bf16[30,256]{1,0:T(8,128)(2,1)S(1)} %slice.281), channel_id=1, source_target_pairs={{0,4},{4,8},{8,12},{12,16},{16,20},{20,24},{24,28},{1,5},{5,9},{9,... | collective-permute-start | bytes 46088 | tf_op jit(solution)/shard_map/ppermute | solution.py:13
  162.4 110.0 %all-to-all-start.1 = ((bf16[8,144,2048]{2,1,0:T(8,128)(2,1)}), bf16[8,144,2048]{2,1,0:T(8,128)(2,1)}, u32[]{:S(2)}, u32[]{:S(2)}) async-start(bf16[8,144,2048]{2,1,0:T(8,128)(2,1)} %bitcast.68), calls=%async_computation.2 | async-start | bytes 9437184 | tf_op jit(solution)/shard_map/all_to_all | solution.py:79
  167.0 139.1 %reduce-scatter.2.cloned.1.call-start = ((), (), s32[]{:S(2)}) async-start(), calls=%async_computation.3 | async-start | bytes 5242880 | tf_op jit(solution)/shard_map/reduce_scatter | solution.py:40
  183.9 0.7 copy-start.4
Sparse Core Ops, SparseCore 0:
  184.1 45.4 reduce-scatter.1
where the time goes:
time: 314 us; the launch traced here: 313 us
  waiting for transfers between devices  182 us (58%)
  local copies, waits for them, and re-layouts  53.2 us (17%)
  matrix products  23.1 us (7%)
  other arithmetic  17.8 us (6%)
  starting transfers between devices  16.2 us (5%)
  between operations  14.2 us (5%)
  blocking collectives  6.75 us (2%)
    all_to_all x1, waiting for transfers between devices, moe_half(): lax.all_to_all(result.reshape(arrived.shape), 'ep', split_axis=0, concat_...  87.7 us
    all_to_all x1, waiting for transfers between devices, moe_half(): lax.all_to_all(send_buffer, 'ep', split_axis=0, concat_axis=0, tiled=True)  64.9 us
    ppermute x1, waiting for transfers between devices, passed_along(): return lax.ppermute(x, axis, pairs)  29.1 us
    gather x1, local copies, waits for them, and re-layouts, moe_half(): padded_in[slot_token].reshape(experts_all, capacity, model_width)  12.3 us
    dot_general x1, matrix products, moe_half(): jnp.dot(inner, expert_down[0], preferred_element_type=jnp.float32)  11 us
    gather x1, local copies, waits for them, and re-layouts, moe_half(): picked = returned_flat[slot_index].reshape(rows, TOP, model_width)  10 us
    slice x1, local copies, waits for them, and re-layouts, moe_half(): picked[:, 0].astype(jnp.float32)  7.65 us
    all_to_all x1, starting transfers between devices, moe_half(): lax.all_to_all(send_buffer, 'ep', split_axis=0, concat_axis=0, tiled=True)  7.41 us
  transfers between devices with their start and end apart: 4, of which 3 were waited for; matrix products, arithmetic and copies ran while one was open for 16% of the time, Pallas kernels for 0%

commit v1 on v0

--- a/solution.py
+++ b/solution.py
@@ -3,7 +3,7 @@
 from jax import lax
 from jax.sharding import PartitionSpec as P
 
-CONV = 1024
+GROUPS = 4
 TOP = 2
 
 
@@ -13,18 +13,21 @@
     return lax.ppermute(x, axis, pairs)
 
 
-def conv_half(conv_value, conv_gate, depth_weight, norm_gain, norm_shift, conv_out_weight):
+def gate_and_halo(conv_value, conv_gate, reach):
+    gated = (conv_value.astype(jnp.float32) * jax.nn.sigmoid(conv_gate.astype(jnp.float32))).astype(
+        jnp.bfloat16
+    )
+    return gated, passed_along(gated[gated.shape[0] - reach :], "ep", 1)
+
+
+def conv_half(conv_value, gated, earlier, depth_weight, norm_gain, norm_shift, conv_out_weight):
     channels = conv_value.shape[1]
     length = conv_value.shape[0]
     first_col = lax.axis_index("tp") * channels
     taps = lax.dynamic_slice_in_dim(depth_weight, first_col, channels, 1)
     gains = lax.dynamic_slice_in_dim(norm_gain, first_col, channels, 0)
     shifts = lax.dynamic_slice_in_dim(norm_shift, first_col, channels, 0)
-    gated = (conv_value.astype(jnp.float32) * jax.nn.sigmoid(conv_gate.astype(jnp.float32))).astype(
-        jnp.bfloat16
-    )
     reach = taps.shape[0] - 1
-    earlier = passed_along(gated[length - reach :], "ep", 1)
     padded = jnp.concatenate([earlier, gated], 0).astype(jnp.float32)
     filtered = taps[0] * padded[0:length]
     for offset in range(1, reach + 1):
@@ -32,8 +35,9 @@
     sums, squares = lax.psum(
         (jnp.sum(filtered, axis=1), jnp.sum(filtered * filtered, axis=1)), "tp"
     )
-    center = (sums / CONV)[:, None]
-    spread = (squares / CONV)[:, None] - center * center
+    all_channels = channels * lax.axis_size("tp")
+    center = (sums / all_channels)[:, None]
+    spread = (squares / all_channels)[:, None] - center * center
     normed = (filtered - center) * lax.rsqrt(spread + 1e-05) * gains + shifts
     activated = jax.nn.silu(normed).astype(jnp.bfloat16)
     partial_value = jnp.dot(activated, conv_out_weight, preferred_element_type=jnp.float32)
@@ -94,6 +98,108 @@
         :, 1
     ].astype(jnp.float32)
     return combined.astype(jnp.bfloat16)
+
+
+def swapped(x, axis, mask):
+    peers = lax.axis_size(axis)
+    return lax.ppermute(x, axis, [(i, i ^ mask) for i in range(peers)])
+
+
+def partner_weights(expert_gate, expert_up, expert_down):
+    peers = lax.axis_size("tp")
+    share = expert_down.shape[1] // peers
+    first = lax.axis_index("tp") * share
+    gate_up = jnp.concatenate(
+        [
+            lax.dynamic_slice_in_dim(expert_gate[0], first, share, 1),
+            lax.dynamic_slice_in_dim(expert_up[0], first, share, 1),
+        ],
+        1,
+    )
+    down = lax.dynamic_slice_in_dim(expert_down[0], first, share, 0)
+    gate_ups = [swapped(gate_up, "ep", 1)]
+    downs = [swapped(down, "ep", 1)]
+    mask = peers // 2
+    while mask:
+        gate_ups = gate_ups + [swapped(piece, "tp", mask) for piece in gate_ups]
+        downs = downs + [swapped(piece, "tp", mask) for piece in downs]
+        mask //= 2
+    gate = jnp.concatenate([piece[:, :share] for piece in gate_ups], 1)
+    up = jnp.concatenate([piece[:, share:] for piece in gate_ups], 1)
+    return gate, up, jnp.concatenate(downs, 0)
+
+
+def one_expert(rows, gate, up, down):
+    gate_act = jnp.dot(rows, gate, preferred_element_type=jnp.float32)
+    up_act = jnp.dot(rows, up, preferred_element_type=jnp.float32)
+    inner = (jax.nn.silu(gate_act) * up_act).astype(jnp.bfloat16)
+    return jnp.dot(inner, down, preferred_element_type=jnp.float32).astype(jnp.bfloat16)
+
+
+def pair_half(moe_input, moe_gain, route_experts, route_scores, expert_gate, expert_up, expert_down, first):
+    rows, model_width = moe_input.shape
+    experts_all = lax.axis_size("ep")
+    groups = experts_all // TOP
+    capacity = 2 * (3 * TOP * rows // (4 * experts_all))
+    other = partner_weights(expert_gate, expert_up, expert_down)
+    widened = moe_input.astype(jnp.float32)
+    normal_in = (
+        widened * lax.rsqrt(jnp.mean(widened * widened, axis=-1, keepdims=True) + 1e-06) * moe_gain
+    ).astype(jnp.bfloat16)
+    row_group = route_experts[:, 0] // TOP
+    onehot = (row_group[:, None] == jnp.arange(groups, dtype=jnp.int32)[None, :]).astype(
+        jnp.bfloat16
+    )
+    order = jnp.arange(rows, dtype=jnp.int32)
+    before = (order[:, None] > order[None, :]).astype(jnp.bfloat16)
+    ranks = jnp.dot(before, onehot, preferred_element_type=jnp.float32)
+    rank = jnp.sum(ranks * onehot.astype(jnp.float32), axis=1).astype(jnp.int32)
+    slot = jnp.where(rank < capacity, row_group * capacity + rank, -1)
+    slots = jnp.arange(groups * capacity, dtype=jnp.int32)
+    pick = (slots[:, None] == slot[None, :]).astype(jnp.bfloat16)
+    group_gate = jax.nn.sigmoid(route_scores[:, 0])
+    first_weight = group_gate * jax.nn.sigmoid(route_scores[:, 1])
+    second_weight = group_gate * jax.nn.sigmoid(-route_scores[:, 1])
+    in_order = route_experts[:, 0] % TOP == 0
+    low_weight = jnp.where(in_order, first_weight, second_weight)
+    high_weight = jnp.where(in_order, second_weight, first_weight)
+    lane = jnp.arange(128, dtype=jnp.int32)[None, :]
+    weights = jnp.where(lane < 64, low_weight[:, None], high_weight[:, None])
+    coarse = lax.reduce_precision(weights, 8, 7)
+    extra = jnp.where(lane % 64 < 32, coarse, weights - coarse).astype(jnp.bfloat16)
+    sent = jnp.dot(
+        pick, jnp.concatenate([normal_in, extra], 1), preferred_element_type=jnp.float32
+    ).astype(jnp.bfloat16)
+    sent, _ = lax.optimization_barrier((sent, first))
+    along = [[TOP * g + x for g in range(groups)] for x in range(TOP)]
+    arrived = lax.all_to_all(
+        sent.reshape(groups, capacity, -1),
+        "ep",
+        split_axis=0,
+        concat_axis=0,
+        axis_index_groups=along,
+        tiled=True,
+    ).reshape(groups * capacity, -1)
+    flat_rows = arrived[:, :model_width]
+    tail = arrived[:, model_width:].astype(jnp.float32)
+    low = tail[:, 0:1] + tail[:, 32:33]
+    high = tail[:, 64:65] + tail[:, 96:97]
+    even = lax.axis_index("ep") % TOP == 0
+    mine = one_expert(flat_rows, expert_gate[0], expert_up[0], expert_down[0])
+    theirs = one_expert(flat_rows, *other)
+    combined = jnp.where(even, low, high) * mine.astype(jnp.float32) + jnp.where(
+        even, high, low
+    ) * theirs.astype(jnp.float32)
+    returned = lax.all_to_all(
+        combined.astype(jnp.bfloat16).reshape(groups, capacity, model_width),
+        "ep",
+        split_axis=0,
+        concat_axis=0,
+        axis_index_groups=along,
+        tiled=True,
+    ).reshape(groups * capacity, model_width)
+    put = (slot[:, None] == slots[None, :]).astype(jnp.bfloat16)
+    return jnp.dot(put, returned, preferred_element_type=jnp.float32).astype(jnp.bfloat16)
 
 
 def on_device(
@@ -111,12 +217,17 @@
     expert_up,
     expert_down,
 ):
+    gated, earlier = gate_and_halo(conv_value, conv_gate, depth_weight.shape[0] - 1)
     conv_out = conv_half(
-        conv_value, conv_gate, depth_weight, norm_gain, norm_shift, conv_out_weight
-    )
-    moe_out = moe_half(
+        conv_value, gated, earlier, depth_weight, norm_gain, norm_shift, conv_out_weight
+    )
+    moe_args = (
         moe_input, moe_gain, route_experts, route_scores, expert_gate, expert_up, expert_down
     )
+    if lax.axis_size("ep") // GROUPS == TOP:
+        moe_out = pair_half(*moe_args, earlier)
+    else:
+        moe_out = moe_half(*moe_args)
     return (conv_out, moe_out)
 
 

time: 314 us -> 192 us (0.61)
  waiting for transfers between devices: 182 us -> 74.4 us
  local copies, waits for them, and re-layouts: 53.2 us -> 14.1 us
  matrix products: 23.1 us -> 37.3 us
  blocking collectives: 6.75 us -> 20 us
  other arithmetic: 17.8 us -> 11 us
  starting transfers between devices: 16.2 us -> 20.1 us
    all_to_all x2, waiting for transfers between devices: 153 us -> 63.8 us  [the longest x1 53.4 us: pair_half(): lax.all_to_all(combined.astype(jnp.bfloat16).reshape(groups, capacity, mo...]
    ppermute x1, waiting for transfers between devices: 29.1 us -> 5.91 us  [passed_along(): return lax.ppermute(x, axis, pairs)]
    gather x2 -> x0, local copies, waits for them, and re-layouts: 22.3 us -> none  [the longest x1 12.3 us: moe_half(): padded_in[slot_token].reshape(experts_all, capacity, model_width)]
    dot_general x2 -> x8, matrix products: 18 us -> 32.7 us  [the longest x2 11.4 us: one_expert(): jnp.dot(inner, down, preferred_element_type=jnp.float32)]
    psum x1, blocking collectives: 6.75 us -> 20 us  [conv_half(): lax.psum((jnp.sum(filtered, axis=1), jnp.sum(filtered * filtered, axis=1)...]
    ppermute x0 -> x8, starting transfers between devices: none -> 8.83 us  [swapped(): return lax.ppermute(x, axis, [(i, i ^ mask) for i in range(peers)])]
    concatenate x2 -> x0, local copies, waits for them, and re-layouts: 6.48 us -> none  [the longest x1 5.18 us: moe_half(): jnp.concatenate([returned.reshape(experts_all * capacity, model_width), j...]
    reshape x1 -> x0, local copies, waits for them, and re-layouts: 6.01 us -> none  [moe_half(): picked = returned_flat[slot_index].reshape(rows, TOP, model_width)]
  transfers between devices with their start and end apart: 4 -> 12, of which waited for: 3 -> 4; matrix products, arithmetic and copies ran while one was open for 16% -> 31% of each run, Pallas kernels for 0% -> 0%
where the time goes in v1:
time: 192 us; the launch traced here: 191 us
  waiting for transfers between devices  74.4 us (39%)
  matrix products  37.3 us (19%)
  starting transfers between devices  20.1 us (10%)
  blocking collectives  20 us (10%)
  between operations  14.4 us (8%)
  local copies, waits for them, and re-layouts  14.1 us (7%)
  other arithmetic  11 us (6%)
    all_to_all x1, waiting for transfers between devices, pair_half(): lax.all_to_all(combined.astype(jnp.bfloat16).reshape(groups, capacity, mo...  53.4 us
    psum x1, blocking collectives, conv_half(): lax.psum((jnp.sum(filtered, axis=1), jnp.sum(filtered * filtered, axis=1)...  20 us
    dot_general x2, matrix products, one_expert(): jnp.dot(inner, down, preferred_element_type=jnp.float32)  11.4 us
    all_to_all x1, waiting for transfers between devices, pair_half(): lax.all_to_all(sent.reshape(groups, capacity, -1), 'ep', split_axis=0, co...  10.4 us
    dot_general x2, matrix products, one_expert(): gate_act = jnp.dot(rows, gate, preferred_element_type=jnp.float32)  8.97 us
    ppermute x8, starting transfers between devices, swapped(): return lax.ppermute(x, axis, [(i, i ^ mask) for i in range(peers)])  8.83 us
    slice x4, local copies, waits for them, and re-layouts, partner_weights(): gate = jnp.concatenate([piece[:, :share] for piece in gate_ups], 1)  8.05 us
    ppermute x1, waiting for transfers between devices, passed_along(): return lax.ppermute(x, axis, pairs)  5.91 us
  transfers between devices with their start and end apart: 12, of which 4 were waited for; matrix products, arithmetic and copies ran while one was open for 31% of the time, Pallas kernels for 0%

profile of v1, /device:TPU:0, one launch (start us, length us, event | category | flops | bytes accessed | tf_op | source)
XLA Modules:
  0.0 191.3 jit_solution(574739405191183080)
XLA Ops:
  9.8 3.0 %collective-permute-start.1 = (bf16[2048,256]{1,0:T(8,128)(2,1)}, bf16[2048,256]{1,0:T(8,128)(2,1)}, u32[]{:S(2)}, u32[]{:S(2)}) collective-permute-start(bf16[2048,256]{1,0:T(8,128)(2,1)} %pad_maximum_fusion), channel_id=1, source_target_pairs={{0,4},{4,0},{8,12},{12,8},{16,20},{20,16},{24,28},{28,24},{1,5},{5... | collective-permute-start | bytes 3145736 | tf_op jit(solution)/shard_map/ppermute | solution.py:105
  13.1 1.9 collective-permute-start
  15.8 3.0 %collective-permute-start.5 = (bf16[128,2048]{1,0:T(8,128)(2,1)}, bf16[128,2048]{1,0:T(8,128)(2,1)}, u32[]{:S(2)}, u32[]{:S(2)}) collective-permute-start(bf16[128,2048]{1,0:T(8,128)(2,1)} %dynamic-slice_bitcast_fusion), channel_id=1, source_target_pairs={{0,4},{4,0},{8,12},{12,8},{16,20},{20,16},{24,28},{28,24},{1,5},{5... | collective-permute-start | bytes 1572872 | tf_op jit(solution)/shard_map/ppermute | solution.py:105
  19.6 3.0 %fusion.2 = bf16[384,2048]{1,0:T(8,128)(2,1)} fusion(bf16[384,2048]{1,0:T(8,128)(2,1)} %param.19, f32[2048]{0:T(1024)S(1)} %copy-done.8, f32[384]{0:T(512)S(1)} %add_rsqrt_fusion.1), kind=kLoop, calls=%fused_computation.7 | loop fusion | flops 3145728 | bytes 3155456 | tf_op jit(solution)/shard_map/convert_element_type | solution.py:148
  23.9 4.4 %convolution_convert_fusion = bf16[576,2176]{1,0:T(8,128)(2,1)} fusion(bf16[384,128]{1,0:T(8,128)(2,1)S(1)} %fusion.92, bf16[384,2048]{1,0:T(8,128)(2,1)} %fusion.2, s32[384]{0:T(512)S(1)} %fusion.98), kind=kOutput, calls=%fused_computation.1 | convolution fusion | flops 967409664 | bytes 4179456 | tf_op jit(solution)/shard_map/dot_general | solution.py:170
  30.9 5.9 %collective-permute-done = bf16[30,256]{1,0:T(8,128)(2,1)S(1)} collective-permute-done((bf16[30,256]{1,0:T(8,128)(2,1)S(1)}, bf16[30,256]{1,0:T(8,128)(2,1)S(1)}, u32[]{:S(2)}, u32[]{:S(2)}) %collective-permute-start) | collective-permute-done | bytes 15392 | tf_op jit(solution)/shard_map/ppermute | solution.py:13
  36.8 4.9 %all-to-all-start = ((bf16[4,144,2176]{2,1,0:T(8,128)(2,1)}), bf16[4,144,2176]{2,1,0:T(8,128)(2,1)}, u32[]{:S(2)}, u32[]{:S(2)}) async-start(bf16[4,144,2176]{2,1,0:T(8,128)(2,1)} %bitcast.58), calls=%async_computation.1 | async-start | bytes 5013504 | tf_op jit(solution)/shard_map/all_to_all | solution.py:175
  41.8 1.6 collective-permute-start.2
  43.4 4.4 %fusion.111 = (f32[1024]{0:T(1024)S(1)}, f32[1024]{0:T(1024)S(1)}, f32[1024,256]{1,0:T(8,128)S(1)}) fusion(f32[1054,256]{1,0:T(8,128)S(1)} %maximum_convert_fusion, f32[256]{0:T(256)S(1)} %bitcast.90, f32[256]{0:T(256)S(1)} %bitcast.61, f32[256]{0:T(256)S(1)} %bitcast.62, f32[256]{0:T(256)S(1)} %bitcast.63, f32[256]{0:T(256)S(1)} %bitcast.64, ...), kind=kLoop, calls=%fused_computation.181 | loop fusion | flops 16775168 | bytes 33594368 | tf_op jit(solution)/shard_map/reduce_sum | solution.py:36
  47.9 20.0 %all-reduce = (f32[1024]{0:T(1024)S(1)}, f32[1024]{0:T(1024)S(1)}) all-reduce(f32[1024]{0:T(1024)S(1)} %get-tuple-element.5, f32[1024]{0:T(1024)S(1)} %get-tuple-element.4), channel_id=1, replica_groups=mesh['ep'=8,'tp'=4] {'tp'}, use_global_device_ids=true, to_apply=%region_3.0 | all-reduce | flops 2048 | bytes 16384 | tf_op jit(solution)/shard_map/psum | solution.py:35
  68.4 4.6 %convolution_convert_fusion.1 = bf16[1024,2048]{1,0:T(8,128)(2,1)} fusion(bf16[256,2048]{1,0:T(8,128)(2,1)} %param.18, f32[1024,256]{1,0:T(8,128)S(1)} %get-tuple-element.17, f32[256]{0:T(256)S(1)} %dynamic_slice.26, f32[256]{0:T(256)S(1)} %dynamic_slice.25, f32[1024]{0:T(1024)S(1)} %get-tuple-element.58, f32[1024]{0:T(1024)S(1)} %get-tuple-element.57), kind=kOutput, calls=%fused_computation.4 | convolution fusion | flops 1078198272 | bytes 6301696 | tf_op jit(solution)/shard_map/dot_general | solution.py:43
  73.7 2.1 %fusion.114 = (bf16[2048,128]{1,0:T(8,128)(2,1)}, bf16[2048,128]{1,0:T(8,128)(2,1)S(1)}) fusion(bf16[2048,256]{1,0:T(8,128)(2,1)} %collective-permute-done.1), kind=kLoop, calls=%fused_computation.183 | loop fusion | bytes 2097152 | tf_op jit(solution)/shard_map/slice | solution.py:127
  75.8 4.6 %collective-permute-done.6 = bf16[128,2048]{1,0:T(8,128)(2,1)} collective-permute-done((bf16[128,2048]{1,0:T(8,128)(2,1)}, bf16[128,2048]{1,0:T(8,128)(2,1)}, u32[]{:S(2)}, u32[]{:S(2)}) %collective-permute-start.6) | collective-permute-done | bytes 524320 | tf_op jit(solution)/shard_map/ppermute | solution.py:105
  80.4 2.4 %fusion.115 = (bf16[2048,128]{1,0:T(8,128)(2,1)}, bf16[2048,128]{1,0:T(8,128)(2,1)S(1)}) fusion(bf16[2048,256]{1,0:T(8,128)(2,1)} %collective-permute-done.2), kind=kLoop, calls=%fused_computation.184 | loop fusion | bytes 2097152 | tf_op jit(solution)/shard_map/slice | solution.py:127
  82.8 2.5 %fusion.116 = (bf16[2048,128]{1,0:T(8,128)(2,1)}, bf16[2048,128]{1,0:T(8,128)(2,1)}) fusion(bf16[2048,256]{1,0:T(8,128)(2,1)} %collective-permute-done.3), kind=kLoop, calls=%fused_computation.185 | loop fusion | bytes 2097152 | tf_op jit(solution)/shard_map/slice | solution.py:127
  86.4 10.4 %all-to-all-done = bf16[4,144,2176]{2,1,0:T(8,128)(2,1)} async-done(((bf16[4,144,2176]{2,1,0:T(8,128)(2,1)}), bf16[4,144,2176]{2,1,0:T(8,128)(2,1)}, u32[]{:S(2)}, u32[]{:S(2)}) %all-to-all-start) | async-done | bytes 2506784 | tf_op jit(solution)/shard_map/all_to_all | solution.py:175
  98.3 4.8 %fusion.29 = f32[576,512]{1,0:T(8,128)} fusion(bf16[1,2048,512]{2,1,0:T(8,128)(2,1)} %param.23, bf16[576,2176]{1,0:T(8,128)(2,1)} %bitcast.32), kind=kOutput, calls=%fused_computation.37 | convolution fusion | flops 1207959552 | bytes 5636096 | tf_op jit(solution)/shard_map/dot_general | solution.py:133
  103.1 4.1 %fusion.3 = f32[576,512]{1,0:T(8,128)} fusion(bf16[2048,128]{1,0:T(8,128)(2,1)S(1)} %copy-done.7, bf16[2048,128]{1,0:T(8,128)(2,1)S(1)} %copy-done.6, bf16[2048,128]{1,0:T(8,128)(2,1)S(1)} %copy-done.5, bf16[2048,128]{1,0:T(8,128)(2,1)S(1)} %copy-done.4, bf16[576,2176]{1,0:T(8,128)(2,1)} %bitcast.32), kind=kOutput, calls=%fused_computation.11 | convolution fusion | flops 1216348160 | bytes 5636096 | tf_op jit(solution)/shard_map/dot_general | solution.py:133
  107.3 6.8 %convolution_convert_fusion.3 = bf16[576,2048]{1,0:T(8,128)(2,1)} fusion(bf16[1,512,2048]{2,1,0:T(8,128)(2,1)S(1)} %copy-done, bf16[1,2048,512]{2,1,0:T(8,128)(2,1)} %param.24, bf16[576,2176]{1,0:T(8,128)(2,1)} %bitcast.32, f32[576,512]{1,0:T(8,128)} %fusion.29), kind=kOutput, calls=%fused_computation.9 | convolution fusion | flops 2418868224 | bytes 10092544 | tf_op jit(solution)/shard_map/dot_general | solution.py:136
  114.1 3.5 %fusion.11 = f32[576,512]{1,0:T(8,128)S(1)} fusion(bf16[2048,128]{1,0:T(8,128)(2,1)} %get-tuple-element.25, bf16[2048,128]{1,0:T(8,128)(2,1)} %get-tuple-element.23, bf16[2048,128]{1,0:T(8,128)(2,1)S(1)} %get-tuple-element.21, bf16[2048,128]{1,0:T(8,128)(2,1)S(1)} %get-tuple-element.19, bf16[576,2176]{1,0:T(8,128)(2,1)} %bitcast.32), kind=kOutput, calls=%fused_computation.19 | convolution fusion | flops 1216348160 | bytes 5636096 | tf_op jit(solution)/shard_map/dot_general | solution.py:134
  117.7 4.5 %add_convert_fusion = bf16[576,2048]{1,0:T(8,128)(2,1)} fusion(bf16[576,2048]{1,0:T(8,128)(2,1)S(1)} %copy-done.11, f32[576]{0:T(1024)S(1)} %get-tuple-element.7, f32[576]{0:T(1024)S(1)} %get-tuple-element.6, bf16[128,2048]{1,0:T(8,128)(2,1)} %collective-permute-done.8, bf16[128,2048]{1,0:T(8,128)(2,1)} %collective-permute-done.7, ...), kind=kOutput, calls=%fused_computation | convolution fusion | flops 1226375168 | bytes 9179648 | tf_op jit(solution)/shard_map/dot_general | solution.py:136
  122.2 4.5 %all-to-all-start.1 = ((bf16[4,144,2048]{2,1,0:T(8,128)(2,1)}), bf16[4,144,2048]{2,1,0:T(8,128)(2,1)}, u32[]{:S(2)}, u32[]{:S(2)}) async-start(bf16[4,144,2048]{2,1,0:T(8,128)(2,1)} %bitcast.59), calls=%async_computation.2 | async-start | bytes 4718592 | tf_op jit(solution)/shard_map/all_to_all | solution.py:193
  126.7 53.4 %all-to-all-done.1 = bf16[4,144,2048]{2,1,0:T(8,128)(2,1)} async-done(((bf16[4,144,2048]{2,1,0:T(8,128)(2,1)}), bf16[4,144,2048]{2,1,0:T(8,128)(2,1)}, u32[]{:S(2)}, u32[]{:S(2)}) %all-to-all-start.1) | async-done | bytes 2359328 | tf_op jit(solution)/shard_map/all_to_all | solution.py:193
  180.2 4.2 %convolution_convert_fusion.4 = bf16[384,2048]{1,0:T(8,128)(2,1)} fusion(bf16[576,2048]{1,0:T(8,128)(2,1)} %bitcast.40, s32[384]{0:T(512)S(1)} %fusion.102), kind=kOutput, calls=%fused_computation.10 | convolution fusion | flops 906977280 | bytes 3933696 | tf_op jit(solution)/shard_map/dot_general | solution.py:202
  (66 shorter events, 12.2 us)
Async XLA Ops:
  7.2 7.8 %copy-start = (bf16[1,512,2048]{2,1,0:T(8,128)(2,1)S(1)}, bf16[1,512,2048]{2,1,0:T(8,128)(2,1)}, u32[]{:S(2)}) copy-start(bf16[1,512,2048]{2,1,0:T(8,128)(2,1)} %param.25) | copy-start | bytes 6291460
  7.2 5.6 %copy-start.2 = (bf16[1024,256]{1,0:T(8,128)(2,1)S(1)}, bf16[1024,256]{1,0:T(8,128)(2,1)}, u32[]{:S(2)}) copy-start(bf16[1024,256]{1,0:T(8,128)(2,1)} %param.14) | copy-start | bytes 1572868
  7.2 5.5 %copy-start.3 = (bf16[1024,256]{1,0:T(8,128)(2,1)S(1)}, bf16[1024,256]{1,0:T(8,128)(2,1)}, u32[]{:S(2)}) copy-start(bf16[1024,256]{1,0:T(8,128)(2,1)} %param.13) | copy-start | bytes 1572868
  8.6 10.2 %copy-start.10 = (s32[384,2]{0,1:T(2,128)S(1)}, s32[384,2]{0,1:T(2,128)}, u32[]{:S(2)}) copy-start(s32[384,2]{0,1:T(2,128)} %param.21) | copy-start | bytes 9220
  8.7 10.3 %copy-start.9 = (f32[384,2]{0,1:T(2,128)S(1)}, f32[384,2]{0,1:T(2,128)}, u32[]{:S(2)}) copy-start(f32[384,2]{0,1:T(2,128)} %param.22) | copy-start | bytes 9220
  8.7 10.5 %copy-start.1 = (bf16[384,2048]{1,0:T(8,128)(2,1)S(1)}, bf16[384,2048]{1,0:T(8,128)(2,1)}, u32[]{:S(2)}) copy-start(bf16[384,2048]{1,0:T(8,128)(2,1)} %param.19) | copy-start | bytes 4718596
  9.8 9.8 %copy-start.8 = (f32[2048]{0:T(1024)S(1)}, f32[2048]{0:T(1024)}, u32[]{:S(2)}) copy-start(f32[2048]{0:T(1024)} %param.20) | copy-start | bytes 24580
  9.8 32.1 %collective-permute-start.1 = (bf16[2048,256]{1,0:T(8,128)(2,1)}, bf16[2048,256]{1,0:T(8,128)(2,1)}, u32[]{:S(2)}, u32[]{:S(2)}) collective-permute-start(bf16[2048,256]{1,0:T(8,128)(2,1)} %pad_maximum_fusion), channel_id=1, source_target_pairs={{0,4},{4,0},{8,12},{12,8},{16,20},{20,16},{24,28},{28,24},{1,5},{5... | collective-permute-start | bytes 3145736 | tf_op jit(solution)/shard_map/ppermute | solution.py:105
  13.1 23.8 %collective-permute-start = (bf16[30,256]{1,0:T(8,128)(2,1)S(1)}, bf16[30,256]{1,0:T(8,128)(2,1)S(1)}, u32[]{:S(2)}, u32[]{:S(2)}) collective-permute-start(bf16[30,256]{1,0:T(8,128)(2,1)S(1)} %slice.322), channel_id=1, source_target_pairs={{0,4},{4,8},{8,12},{12,16},{16,20},{20,24},{24,28},{1,5},{5,9},{9,... | collective-permute-start | bytes 46088 | tf_op jit(solution)/shard_map/ppermute | solution.py:13
  15.8 52.0 %collective-permute-start.5 = (bf16[128,2048]{1,0:T(8,128)(2,1)}, bf16[128,2048]{1,0:T(8,128)(2,1)}, u32[]{:S(2)}, u32[]{:S(2)}) collective-permute-start(bf16[128,2048]{1,0:T(8,128)(2,1)} %dynamic-slice_bitcast_fusion), channel_id=1, source_target_pairs={{0,4},{4,0},{8,12},{12,8},{16,20},{20,16},{24,28},{28,24},{1,5},{5... | collective-permute-start | bytes 1572872 | tf_op jit(solution)/shard_map/ppermute | solution.py:105
  36.8 60.0 %all-to-all-start = ((bf16[4,144,2176]{2,1,0:T(8,128)(2,1)}), bf16[4,144,2176]{2,1,0:T(8,128)(2,1)}, u32[]{:S(2)}, u32[]{:S(2)}) async-start(bf16[4,144,2176]{2,1,0:T(8,128)(2,1)} %bitcast.58), calls=%async_computation.1 | async-start | bytes 5013504 | tf_op jit(solution)/shard_map/all_to_all | solution.py:175
  41.7 142.7 %reduce-scatter.2.cloned.1.call-start = ((), (), s32[]{:S(2)}) async-start(), calls=%async_computation.3 | async-start | bytes 5242880 | tf_op jit(solution)/shard_map/reduce_scatter | solution.py:44
  41.8 31.8 %collective-permute-start.2 = (bf16[2048,256]{1,0:T(8,128)(2,1)}, bf16[2048,256]{1,0:T(8,128)(2,1)}, u32[]{:S(2)}, u32[]{:S(2)}) collective-permute-start(bf16[2048,256]{1,0:T(8,128)(2,1)} %collective-permute-done.1), channel_id=1, source_target_pairs={{0,2},{1,3},{2,0},{3,1},{4,6},{5,7},{6,4},{7,5},{8,10},{9,11},{10,... | collective-permute-start | bytes 3145736 | tf_op jit(solution)/shard_map/ppermute | solution.py:105
  67.9 12.5 %collective-permute-start.6 = (bf16[128,2048]{1,0:T(8,128)(2,1)}, bf16[128,2048]{1,0:T(8,128)(2,1)}, u32[]{:S(2)}, u32[]{:S(2)}) collective-permute-start(bf16[128,2048]{1,0:T(8,128)(2,1)} %collective-permute-done.5), channel_id=1, source_target_pairs={{0,2},{1,3},{2,0},{3,1},{4,6},{5,7},{6,4},{7,5},{8,10},{9,11},{10,... | collective-permute-start | bytes 1572872 | tf_op jit(solution)/shard_map/ppermute | solution.py:105
  68.4 14.4 %collective-permute-start.3 = (bf16[2048,256]{1,0:T(8,128)(2,1)}, bf16[2048,256]{1,0:T(8,128)(2,1)}, u32[]{:S(2)}, u32[]{:S(2)}) collective-permute-start(bf16[2048,256]{1,0:T(8,128)(2,1)} %collective-permute-done.1), channel_id=1, source_target_pairs={{0,1},{1,0},{2,3},{3,2},{4,5},{5,4},{6,7},{7,6},{8,9},{9,8},{10,11... | collective-permute-start | bytes 3145736 | tf_op jit(solution)/shard_map/ppermute | solution.py:105
  73.0 44.6 %collective-permute-start.7 = (bf16[128,2048]{1,0:T(8,128)(2,1)}, bf16[128,2048]{1,0:T(8,128)(2,1)}, u32[]{:S(2)}, u32[]{:S(2)}) collective-permute-start(bf16[128,2048]{1,0:T(8,128)(2,1)} %collective-permute-done.5), channel_id=1, source_target_pairs={{0,1},{1,0},{2,3},{3,2},{4,5},{5,4},{6,7},{7,6},{8,9},{9,8},{10,11... | collective-permute-start | bytes 1572872 | tf_op jit(solution)/shard_map/ppermute | solution.py:105
  73.6 11.7 %collective-permute-start.4 = (bf16[2048,256]{1,0:T(8,128)(2,1)}, bf16[2048,256]{1,0:T(8,128)(2,1)S(1)}, u32[]{:S(2)}, u32[]{:S(2)}) collective-permute-start(bf16[2048,256]{1,0:T(8,128)(2,1)} %collective-permute-done.2), channel_id=1, source_target_pairs={{0,1},{1,0},{2,3},{3,2},{4,5},{5,4},{6,7},{7,6},{8,9},{9,8},{10,11... | collective-permute-start | bytes 3145736 | tf_op jit(solution)/shard_map/ppermute | solution.py:105
  80.4 37.2 %collective-permute-start.8 = (bf16[128,2048]{1,0:T(8,128)(2,1)}, bf16[128,2048]{1,0:T(8,128)(2,1)}, u32[]{:S(2)}, u32[]{:S(2)}) collective-permute-start(bf16[128,2048]{1,0:T(8,128)(2,1)} %collective-permute-done.6), channel_id=1, source_target_pairs={{0,1},{1,0},{2,3},{3,2},{4,5},{5,4},{6,7},{7,6},{8,9},{9,8},{10,11... | collective-permute-start | bytes 1572872 | tf_op jit(solution)/shard_map/ppermute | solution.py:105
  98.2 4.9 %copy-start.4 = (bf16[2048,128]{1,0:T(8,128)(2,1)S(1)}, bf16[2048,128]{1,0:T(8,128)(2,1)}, u32[]{:S(2)}) copy-start(bf16[2048,128]{1,0:T(8,128)(2,1)} %get-tuple-element.18) | copy-start | bytes 1572868
  98.3 4.9 %copy-start.5 = (bf16[2048,128]{1,0:T(8,128)(2,1)S(1)}, bf16[2048,128]{1,0:T(8,128)(2,1)}, u32[]{:S(2)}) copy-start(bf16[2048,128]{1,0:T(8,128)(2,1)} %get-tuple-element.20) | copy-start | bytes 1572868
  98.3 4.9 %copy-start.6 = (bf16[2048,128]{1,0:T(8,128)(2,1)S(1)}, bf16[2048,128]{1,0:T(8,128)(2,1)}, u32[]{:S(2)}) copy-start(bf16[2048,128]{1,0:T(8,128)(2,1)} %get-tuple-element.22) | copy-start | bytes 1572868
  98.3 4.9 %copy-start.7 = (bf16[2048,128]{1,0:T(8,128)(2,1)S(1)}, bf16[2048,128]{1,0:T(8,128)(2,1)}, u32[]{:S(2)}) copy-start(bf16[2048,128]{1,0:T(8,128)(2,1)} %get-tuple-element.24) | copy-start | bytes 1572868
  114.1 3.5 %copy-start.12 = (f32[576,512]{1,0:T(8,128)S(1)}, f32[576,512]{1,0:T(8,128)}, u32[]{:S(2)}) copy-start(f32[576,512]{1,0:T(8,128)} %fusion.3) | copy-start | bytes 3538948
  122.2 58.0 %all-to-all-start.1 = ((bf16[4,144,2048]{2,1,0:T(8,128)(2,1)}), bf16[4,144,2048]{2,1,0:T(8,128)(2,1)}, u32[]{:S(2)}, u32[]{:S(2)}) async-start(bf16[4,144,2048]{2,1,0:T(8,128)(2,1)} %bitcast.59), calls=%async_computation.2 | async-start | bytes 4718592 | tf_op jit(solution)/shard_map/all_to_all | solution.py:193
  (1 other events, 3.5 us)
Sparse Core Ops, SparseCore 0:
  73.2 47.0 reduce-scatter.1

commit v2 on v1

--- a/solution.py
+++ b/solution.py
@@ -13,14 +13,13 @@
     return lax.ppermute(x, axis, pairs)
 
 
-def gate_and_halo(conv_value, conv_gate, reach):
-    gated = (conv_value.astype(jnp.float32) * jax.nn.sigmoid(conv_gate.astype(jnp.float32))).astype(
+def gated_rows(value, gate):
+    return (value.astype(jnp.float32) * jax.nn.sigmoid(gate.astype(jnp.float32))).astype(
         jnp.bfloat16
     )
-    return gated, passed_along(gated[gated.shape[0] - reach :], "ep", 1)
-
-
-def conv_half(conv_value, gated, earlier, depth_weight, norm_gain, norm_shift, conv_out_weight):
+
+
+def conv_half(conv_value, conv_gate, earlier, depth_weight, norm_gain, norm_shift, conv_out_weight):
     channels = conv_value.shape[1]
     length = conv_value.shape[0]
     first_col = lax.axis_index("tp") * channels
@@ -28,6 +27,7 @@
     gains = lax.dynamic_slice_in_dim(norm_gain, first_col, channels, 0)
     shifts = lax.dynamic_slice_in_dim(norm_shift, first_col, channels, 0)
     reach = taps.shape[0] - 1
+    gated = gated_rows(conv_value, conv_gate)
     padded = jnp.concatenate([earlier, gated], 0).astype(jnp.float32)
     filtered = taps[0] * padded[0:length]
     for offset in range(1, reach + 1):
@@ -41,12 +41,18 @@
     normed = (filtered - center) * lax.rsqrt(spread + 1e-05) * gains + shifts
     activated = jax.nn.silu(normed).astype(jnp.bfloat16)
     partial_value = jnp.dot(activated, conv_out_weight, preferred_element_type=jnp.float32)
-    return lax.psum_scatter(
-        partial_value.astype(jnp.bfloat16).astype(jnp.float32).astype(jnp.bfloat16),
-        "tp",
-        scatter_dimension=0,
-        tiled=True,
-    )
+    return partial_value.astype(jnp.bfloat16)
+
+
+def scattered_sum(partial):
+    peers = lax.axis_size("tp")
+    me = lax.axis_index("tp")
+    size = partial.shape[0] // peers
+    total = lax.dynamic_slice_in_dim(partial, me * size, size, 0).astype(jnp.float32)
+    for mask in range(peers - 1, 0, -1):
+        block = lax.dynamic_slice_in_dim(partial, (me ^ mask) * size, size, 0)
+        total = total + swapped(block, "tp", mask).astype(jnp.float32)
+    return total.astype(jnp.bfloat16)
 
 
 def moe_half(moe_input, moe_gain, route_experts, route_scores, expert_gate, expert_up, expert_down):
@@ -105,10 +111,10 @@
     return lax.ppermute(x, axis, [(i, i ^ mask) for i in range(peers)])
 
 
-def partner_weights(expert_gate, expert_up, expert_down):
+def partner_weights(expert_gate, expert_up, expert_down, place):
     peers = lax.axis_size("tp")
     share = expert_down.shape[1] // peers
-    first = lax.axis_index("tp") * share
+    first = place * share
     gate_up = jnp.concatenate(
         [
             lax.dynamic_slice_in_dim(expert_gate[0], first, share, 1),
@@ -136,12 +142,11 @@
     return jnp.dot(inner, down, preferred_element_type=jnp.float32).astype(jnp.bfloat16)
 
 
-def pair_half(moe_input, moe_gain, route_experts, route_scores, expert_gate, expert_up, expert_down, first):
+def pair_half(moe_input, moe_gain, route_experts, route_scores, expert_gate, expert_up, expert_down, first, beside):
     rows, model_width = moe_input.shape
     experts_all = lax.axis_size("ep")
     groups = experts_all // TOP
     capacity = 2 * (3 * TOP * rows // (4 * experts_all))
-    other = partner_weights(expert_gate, expert_up, expert_down)
     widened = moe_input.astype(jnp.float32)
     normal_in = (
         widened * lax.rsqrt(jnp.mean(widened * widened, axis=-1, keepdims=True) + 1e-06) * moe_gain
@@ -170,7 +175,8 @@
     sent = jnp.dot(
         pick, jnp.concatenate([normal_in, extra], 1), preferred_element_type=jnp.float32
     ).astype(jnp.bfloat16)
-    sent, _ = lax.optimization_barrier((sent, first))
+    sent, _, place = lax.optimization_barrier((sent, first, lax.axis_index("tp")))
+    other = partner_weights(expert_gate, expert_up, expert_down, place)
     along = [[TOP * g + x for g in range(groups)] for x in range(TOP)]
     arrived = lax.all_to_all(
         sent.reshape(groups, capacity, -1),
@@ -180,6 +186,7 @@
         axis_index_groups=along,
         tiled=True,
     ).reshape(groups * capacity, -1)
+    arrived, beside = lax.optimization_barrier((arrived, beside))
     flat_rows = arrived[:, :model_width]
     tail = arrived[:, model_width:].astype(jnp.float32)
     low = tail[:, 0:1] + tail[:, 32:33]
@@ -199,7 +206,8 @@
         tiled=True,
     ).reshape(groups * capacity, model_width)
     put = (slot[:, None] == slots[None, :]).astype(jnp.bfloat16)
-    return jnp.dot(put, returned, preferred_element_type=jnp.float32).astype(jnp.bfloat16)
+    moe_out = jnp.dot(put, returned, preferred_element_type=jnp.float32).astype(jnp.bfloat16)
+    return moe_out, beside
 
 
 def on_device(
@@ -217,18 +225,19 @@
     expert_up,
     expert_down,
 ):
-    gated, earlier = gate_and_halo(conv_value, conv_gate, depth_weight.shape[0] - 1)
-    conv_out = conv_half(
-        conv_value, gated, earlier, depth_weight, norm_gain, norm_shift, conv_out_weight
+    last = conv_value.shape[0] - depth_weight.shape[0] + 1
+    earlier = passed_along(gated_rows(conv_value[last:], conv_gate[last:]), "ep", 1)
+    partial = conv_half(
+        conv_value, conv_gate, earlier, depth_weight, norm_gain, norm_shift, conv_out_weight
     )
     moe_args = (
         moe_input, moe_gain, route_experts, route_scores, expert_gate, expert_up, expert_down
     )
     if lax.axis_size("ep") // GROUPS == TOP:
-        moe_out = pair_half(*moe_args, earlier)
+        moe_out, partial = pair_half(*moe_args, earlier, partial)
     else:
         moe_out = moe_half(*moe_args)
-    return (conv_out, moe_out)
+    return (scattered_sum(partial), moe_out)
 
 
 def solution(mesh):

time: 192 us -> 176 us (0.917)
  between operations: 14.4 us -> 0.93 us
  waiting for transfers between devices: 74.4 us -> 66.2 us
  other arithmetic: 11 us -> 16.9 us
  matrix products: 37.3 us -> 34.8 us
    ppermute x8 -> x11, waiting for transfers between devices: 4.66 us -> 64.8 us  [swapped(): return lax.ppermute(x, axis, [(i, i ^ mask) for i in range(peers)])]
    all_to_all x1, waiting for transfers between devices: 53.4 us -> 1.43 us  [pair_half(): lax.all_to_all(combined.astype(jnp.bfloat16).reshape(groups, capacity, mo...]
    all_to_all x1, waiting for transfers between devices: 10.4 us -> 0.01 us  [pair_half(): lax.all_to_all(sent.reshape(groups, capacity, -1), 'ep', split_axis=0, co...]
    ppermute x1, waiting for transfers between devices: 5.91 us -> 0.01 us  [passed_along(): return lax.ppermute(x, axis, pairs)]
    convert_element_type x1 -> x3, other arithmetic: 0.3 us -> 5.19 us  [the longest x1 2.9 us: scattered_sum(): return total.astype(jnp.bfloat16)]
    dynamic_slice x0 -> x2, local copies, waits for them, and re-layouts: none -> 3.32 us  [the longest x1 2.24 us: scattered_sum(): block = lax.dynamic_slice_in_dim(partial, (me ^ mask) * size, size, 0)]
    ppermute x1, starting transfers between devices: 1.91 us -> 5 us  [passed_along(): return lax.ppermute(x, axis, pairs)]
    slice x4, local copies, waits for them, and re-layouts: 8.05 us -> 5.62 us  [partner_weights(): gate = jnp.concatenate([piece[:, :share] for piece in gate_ups], 1)]
  transfers between devices with their start and end apart: 12 -> 14, of which waited for: 4 -> 5; matrix products, arithmetic and copies ran while one was open for 31% -> 31% of each run, Pallas kernels for 0% -> 0%
where the time goes in v2:
time: 176 us; the launch traced here: 175 us
  waiting for transfers between devices  66.2 us (38%)
  matrix products  34.8 us (20%)
  starting transfers between devices  21.3 us (12%)
  blocking collectives  19.7 us (11%)
  other arithmetic  16.9 us (10%)
  local copies, waits for them, and re-layouts  14.9 us (8%)
    ppermute x11, waiting for transfers between devices, swapped(): return lax.ppermute(x, axis, [(i, i ^ mask) for i in range(peers)])  64.8 us
    psum x1, blocking collectives, conv_half(): lax.psum((jnp.sum(filtered, axis=1), jnp.sum(filtered * filtered, axis=1)...  19.7 us
    dot_general x2, matrix products, one_expert(): jnp.dot(inner, down, preferred_element_type=jnp.float32)  11.3 us
    dot_general x2, matrix products, one_expert(): gate_act = jnp.dot(rows, gate, preferred_element_type=jnp.float32)  8.26 us
    ppermute x11, starting transfers between devices, swapped(): return lax.ppermute(x, axis, [(i, i ^ mask) for i in range(peers)])  6.92 us
    slice x4, local copies, waits for them, and re-layouts, partner_weights(): gate = jnp.concatenate([piece[:, :share] for piece in gate_ups], 1)  5.62 us
    ppermute x1, starting transfers between devices, passed_along(): return lax.ppermute(x, axis, pairs)  5 us
    all_to_all x1, starting transfers between devices, pair_half(): lax.all_to_all(combined.astype(jnp.bfloat16).reshape(groups, capacity, mo...  4.8 us
  transfers between devices with their start and end apart: 14, of which 5 were waited for; matrix products, arithmetic and copies ran while one was open for 31% of the time, Pallas kernels for 0%

profile of v2, /device:TPU:0, one launch (start us, length us, event | category | flops | bytes accessed | tf_op | source)
XLA Modules:
  0.0 174.7 jit_solution(7208101400824003886)
XLA Ops:
  1.6 5.0 %collective-permute-start = (bf16[30,256]{1,0:T(8,128)(2,1)S(1)}, bf16[30,256]{1,0:T(8,128)(2,1)S(1)}, u32[]{:S(2)}, u32[]{:S(2)}) collective-permute-start(bf16[30,256]{1,0:T(8,128)(2,1)S(1)} %multiply_convert_fusion.5), channel_id=1, source_target_pairs={{0,4},{4,8},{8,12},{12,16},{16,20},{20,24},{24,28},{1,5},{5,9},{9,... | collective-permute-start | bytes 46088 | tf_op jit(solution)/shard_map/ppermute | solution.py:13
  8.3 1.8 %fusion = f32[384]{0:T(512)S(1)} fusion(bf16[384,2048]{1,0:T(8,128)(2,1)} %param.19), kind=kLoop, calls=%fused_computation.5 | loop fusion | flops 2358912 | bytes 1574400 | tf_op jit(solution)/shard_map/reduce_sum | solution.py:152
  11.5 3.0 %convolution_convert_fusion = bf16[576,2176]{1,0:T(8,128)(2,1)} fusion(bf16[384,128]{1,0:T(8,128)(2,1)S(1)} %fusion.92, bf16[384,2048]{1,0:T(8,128)(2,1)S(1)} %fusion.2, s32[384]{0:T(512)S(1)} %fusion.98), kind=kOutput, calls=%fused_computation.1 | convolution fusion | flops 967409664 | bytes 4179456 | tf_op jit(solution)/shard_map/dot_general | solution.py:175
  17.8 1.6 collective-permute-start.4
  24.7 4.5 %all-to-all-start = ((bf16[4,144,2176]{2,1,0:T(8,128)(2,1)}), bf16[4,144,2176]{2,1,0:T(8,128)(2,1)}, u32[]{:S(2)}, u32[]{:S(2)}) async-start(bf16[4,144,2176]{2,1,0:T(8,128)(2,1)} %bitcast.58), calls=%async_computation | async-start | bytes 5013504 | tf_op jit(solution)/shard_map/all_to_all | solution.py:181
  31.0 13.2 %collective-permute-done.4 = bf16[2048,256]{1,0:T(8,128)(2,1)} collective-permute-done((bf16[2048,256]{1,0:T(8,128)(2,1)}, bf16[2048,256]{1,0:T(8,128)(2,1)}, u32[]{:S(2)}, u32[]{:S(2)}) %collective-permute-start.4) | collective-permute-done | bytes 1048608 | tf_op jit(solution)/shard_map/ppermute | solution.py:111
  44.2 1.5 collective-permute-start.5
  45.7 4.4 %fusion.111 = (f32[1024]{0:T(1024)S(1)}, f32[1024]{0:T(1024)S(1)}, f32[1024,256]{1,0:T(8,128)S(1)}) fusion(f32[1054,256]{1,0:T(8,128)S(1)} %maximum_convert_fusion, f32[256]{0:T(256)S(1)} %bitcast.72, f32[256]{0:T(256)S(1)} %bitcast.74, f32[256]{0:T(256)S(1)} %bitcast.75, f32[256]{0:T(256)S(1)} %bitcast.76, f32[256]{0:T(256)S(1)} %bitcast.77, ...), kind=kLoop, calls=%fused_computation.186 | loop fusion | flops 16775168 | bytes 33594368 | tf_op jit(solution)/shard_map/reduce_sum | solution.py:36
  50.1 19.7 %all-reduce = (f32[1024]{0:T(1024)S(1)}, f32[1024]{0:T(1024)S(1)}) all-reduce(f32[1024]{0:T(1024)S(1)} %get-tuple-element.11, f32[1024]{0:T(1024)S(1)} %get-tuple-element.10), channel_id=1, replica_groups=mesh['ep'=8,'tp'=4] {'tp'}, use_global_device_ids=true, to_apply=%region_5.6 | all-reduce | flops 2048 | bytes 16384 | tf_op jit(solution)/shard_map/psum | solution.py:35
  70.4 4.6 %convolution_convert_fusion.1 = bf16[1024,2048]{1,0:T(8,128)(2,1)} fusion(bf16[256,2048]{1,0:T(8,128)(2,1)} %param.18, f32[1024,256]{1,0:T(8,128)S(1)} %get-tuple-element.18, f32[256]{0:T(256)S(1)} %dynamic_slice.38, f32[256]{0:T(256)S(1)} %dynamic_slice.37, f32[1024]{0:T(1024)S(1)} %get-tuple-element.67, f32[1024]{0:T(1024)S(1)} %get-tuple-element.66), kind=kOutput, calls=%fused_computation.4 | convolution fusion | flops 1078198272 | bytes 6301696 | tf_op jit(solution)/shard_map/dot_general | solution.py:43
  76.8 5.6 %collective-permute-done.9 = bf16[128,2048]{1,0:T(8,128)(2,1)} collective-permute-done((bf16[128,2048]{1,0:T(8,128)(2,1)}, bf16[128,2048]{1,0:T(8,128)(2,1)}, u32[]{:S(2)}, u32[]{:S(2)}) %collective-permute-start.9) | collective-permute-done | bytes 524320 | tf_op jit(solution)/shard_map/ppermute | solution.py:111
  82.4 2.3 %fusion.115 = (bf16[2048,128]{1,0:T(8,128)(2,1)}, bf16[2048,128]{1,0:T(8,128)(2,1)}) fusion(bf16[2048,256]{1,0:T(8,128)(2,1)} %collective-permute-done.5), kind=kLoop, calls=%fused_computation.189 | loop fusion | bytes 2097152 | tf_op jit(solution)/shard_map/slice | solution.py:133
  86.8 4.7 %fusion.29 = f32[576,512]{1,0:T(8,128)} fusion(bf16[1,2048,512]{2,1,0:T(8,128)(2,1)} %param.23, bf16[576,2176]{1,0:T(8,128)(2,1)} %bitcast.1), kind=kOutput, calls=%fused_computation.37 | convolution fusion | flops 1207959552 | bytes 5636096 | tf_op jit(solution)/shard_map/dot_general | solution.py:139
  92.4 6.8 %convolution_convert_fusion.3 = bf16[576,2048]{1,0:T(8,128)(2,1)} fusion(bf16[1,512,2048]{2,1,0:T(8,128)(2,1)S(1)} %copy-done, bf16[1,2048,512]{2,1,0:T(8,128)(2,1)} %param.24, bf16[576,2176]{1,0:T(8,128)(2,1)} %bitcast.1, f32[576,512]{1,0:T(8,128)} %fusion.29), kind=kOutput, calls=%fused_computation.9 | convolution fusion | flops 2418868224 | bytes 10092544 | tf_op jit(solution)/shard_map/dot_general | solution.py:142
  99.7 3.6 %fusion.3 = f32[576,512]{1,0:T(8,128)S(1)} fusion(bf16[2048,128]{1,0:T(8,128)(2,1)} %get-tuple-element.33, bf16[2048,128]{1,0:T(8,128)(2,1)} %get-tuple-element.31, bf16[2048,128]{1,0:T(8,128)(2,1)} %get-tuple-element.29, bf16[2048,128]{1,0:T(8,128)(2,1)S(1)} %get-tuple-element.27, bf16[576,2176]{1,0:T(8,128)(2,1)} %bitcast.1), kind=kOutput, calls=%fused_computation.11 | convolution fusion | flops 1216348160 | bytes 5636096 | tf_op jit(solution)/shard_map/dot_general | solution.py:139
  103.3 3.2 %fusion.11 = f32[576,512]{1,0:T(8,128)S(1)} fusion(bf16[2048,128]{1,0:T(8,128)(2,1)S(1)} %copy-done.5, bf16[2048,128]{1,0:T(8,128)(2,1)S(1)} %copy-done.4, bf16[2048,128]{1,0:T(8,128)(2,1)S(1)} %copy-done.3, bf16[2048,128]{1,0:T(8,128)(2,1)S(1)} %get-tuple-element.28, bf16[576,2176]{1,0:T(8,128)(2,1)} %bitcast.1), kind=kOutput, calls=%fused_computation.19 | convolution fusion | flops 1216348160 | bytes 5636096 | tf_op jit(solution)/shard_map/dot_general | solution.py:140
  106.6 4.6 %add_convert_fusion = bf16[576,2048]{1,0:T(8,128)(2,1)} fusion(bf16[576,2048]{1,0:T(8,128)(2,1)S(1)} %copy-done.7, f32[576]{0:T(1024)S(1)} %get-tuple-element.13, f32[576]{0:T(1024)S(1)} %get-tuple-element.12, bf16[128,2048]{1,0:T(8,128)(2,1)} %collective-permute-done.11, bf16[128,2048]{1,0:T(8,128)(2,1)} %collective-permute-done.10, ...), kind=kOutput, calls=%fused_computation | convolution fusion | flops 1226375168 | bytes 9179648 | tf_op jit(solution)/shard_map/dot_general | solution.py:142
  111.1 4.8 %all-to-all-start.1 = ((bf16[4,144,2048]{2,1,0:T(8,128)(2,1)}), bf16[4,144,2048]{2,1,0:T(8,128)(2,1)}, u32[]{:S(2)}, u32[]{:S(2)}) async-start(bf16[4,144,2048]{2,1,0:T(8,128)(2,1)} %bitcast.59), calls=%async_computation.1 | async-start | bytes 4718592 | tf_op jit(solution)/shard_map/all_to_all | solution.py:200
  115.9 2.2 %constant_dynamic-slice_fusion.3 = (bf16[256,2048]{1,0:T(8,128)(2,1)S(1)}, bf16[256,2048]{1,0:T(8,128)(2,1)S(1)}, bf16[256,2048]{1,0:T(8,128)(2,1)S(1)}) fusion(bf16[1024,2048]{1,0:T(8,128)(2,1)} %convolution_convert_fusion.1, s32[]{:T(128)S(6)} %select_n.109, s32[]{:T(128)S(6)} %select_n.111, s32[]{:T(128)S(6)} %select_n.110), kind=kLoop, calls=%fused_computation.167 | loop fusion | bytes 6291468 | tf_op jit(solution)/shard_map/dynamic_slice | solution.py:53
  118.2 1.4 collective-permute-start.1
  120.1 23.1 %collective-permute-done.1 = bf16[256,2048]{1,0:T(8,128)(2,1)S(1)} collective-permute-done((bf16[256,2048]{1,0:T(8,128)(2,1)S(1)}, bf16[256,2048]{1,0:T(8,128)(2,1)S(1)}, u32[]{:S(2)}, u32[]{:S(2)}) %collective-permute-start.1) | collective-permute-done | bytes 1048608 | tf_op jit(solution)/shard_map/ppermute | solution.py:111
  143.2 22.9 %collective-permute-done.2 = bf16[256,2048]{1,0:T(8,128)(2,1)S(1)} collective-permute-done((bf16[256,2048]{1,0:T(8,128)(2,1)S(1)}, bf16[256,2048]{1,0:T(8,128)(2,1)S(1)}, u32[]{:S(2)}, u32[]{:S(2)}) %collective-permute-start.2) | collective-permute-done | bytes 1048608 | tf_op jit(solution)/shard_map/ppermute | solution.py:111
  166.2 2.9 %add_convert_fusion.1 = bf16[256,2048]{1,0:T(8,128)(2,1)} fusion(bf16[256,2048]{1,0:T(8,128)(2,1)S(1)} %collective-permute-done.3, bf16[256,2048]{1,0:T(8,128)(2,1)S(1)} %collective-permute-done.2, bf16[256,2048]{1,0:T(8,128)(2,1)S(1)} %collective-permute-done.1, bf16[1024,2048]{1,0:T(8,128)(2,1)} %convolution_convert_fusion.1, s32[]{:T(128)S(6)} %select_n.108), kind=kLoop, calls=%fused_computation.39 | loop fusion | flops 4194304 | bytes 5242884 | tf_op jit(solution)/shard_map/convert_element_type | solution.py:55
  170.5 4.2 %convolution_convert_fusion.4 = bf16[384,2048]{1,0:T(8,128)(2,1)} fusion(bf16[576,2048]{1,0:T(8,128)(2,1)} %bitcast.40, s32[384]{0:T(512)S(1)} %fusion.102), kind=kOutput, calls=%fused_computation.10 | convolution fusion | flops 906977280 | bytes 3933696 | tf_op jit(solution)/shard_map/dot_general | solution.py:209
  (62 shorter events, 22.2 us)
Async XLA Ops:
  0.6 28.6 %copy-start = (bf16[1,512,2048]{2,1,0:T(8,128)(2,1)S(1)}, bf16[1,512,2048]{2,1,0:T(8,128)(2,1)}, u32[]{:S(2)}) copy-start(bf16[1,512,2048]{2,1,0:T(8,128)(2,1)} %param.25) | copy-start | bytes 6291460
  0.6 9.5 %copy-start.1 = (bf16[384,2048]{1,0:T(8,128)(2,1)S(1)}, bf16[384,2048]{1,0:T(8,128)(2,1)}, u32[]{:S(2)}) copy-start(bf16[384,2048]{1,0:T(8,128)(2,1)} %param.19) | copy-start | bytes 4718596
  1.6 12.9 %collective-permute-start = (bf16[30,256]{1,0:T(8,128)(2,1)S(1)}, bf16[30,256]{1,0:T(8,128)(2,1)S(1)}, u32[]{:S(2)}, u32[]{:S(2)}) collective-permute-start(bf16[30,256]{1,0:T(8,128)(2,1)S(1)} %multiply_convert_fusion.5), channel_id=1, source_target_pairs={{0,4},{4,8},{8,12},{12,16},{16,20},{20,24},{24,28},{1,5},{5,9},{9,... | collective-permute-start | bytes 46088 | tf_op jit(solution)/shard_map/ppermute | solution.py:13
  8.3 3.0 %copy-start.6 = (f32[384,2]{0,1:T(2,128)S(1)}, f32[384,2]{0,1:T(2,128)}, u32[]{:S(2)}) copy-start(f32[384,2]{0,1:T(2,128)} %param.22) | copy-start | bytes 9220
  14.5 8.8 %copy-start.2 = (bf16[1024,256]{1,0:T(8,128)(2,1)S(1)}, bf16[1024,256]{1,0:T(8,128)(2,1)}, u32[]{:S(2)}) copy-start(bf16[1024,256]{1,0:T(8,128)(2,1)} %param.14) | copy-start | bytes 1572868
  17.8 26.3 %collective-permute-start.4 = (bf16[2048,256]{1,0:T(8,128)(2,1)}, bf16[2048,256]{1,0:T(8,128)(2,1)}, u32[]{:S(2)}, u32[]{:S(2)}) collective-permute-start(bf16[2048,256]{1,0:T(8,128)(2,1)} %pad_maximum_fusion), channel_id=1, source_target_pairs={{0,4},{4,0},{8,12},{12,8},{16,20},{20,16},{24,28},{28,24},{1,5},{5... | collective-permute-start | bytes 3145736 | tf_op jit(solution)/shard_map/ppermute | solution.py:111
  24.7 62.1 %all-to-all-start = ((bf16[4,144,2176]{2,1,0:T(8,128)(2,1)}), bf16[4,144,2176]{2,1,0:T(8,128)(2,1)}, u32[]{:S(2)}, u32[]{:S(2)}) async-start(bf16[4,144,2176]{2,1,0:T(8,128)(2,1)} %bitcast.58), calls=%async_computation | async-start | bytes 5013504 | tf_op jit(solution)/shard_map/all_to_all | solution.py:181
  30.1 39.7 %collective-permute-start.8 = (bf16[128,2048]{1,0:T(8,128)(2,1)}, bf16[128,2048]{1,0:T(8,128)(2,1)}, u32[]{:S(2)}, u32[]{:S(2)}) collective-permute-start(bf16[128,2048]{1,0:T(8,128)(2,1)} %dynamic-slice_bitcast_fusion), channel_id=1, source_target_pairs={{0,4},{4,0},{8,12},{12,8},{16,20},{20,16},{24,28},{28,24},{1,5},{5... | collective-permute-start | bytes 1572872 | tf_op jit(solution)/shard_map/ppermute | solution.py:111
  44.2 31.4 %collective-permute-start.5 = (bf16[2048,256]{1,0:T(8,128)(2,1)}, bf16[2048,256]{1,0:T(8,128)(2,1)}, u32[]{:S(2)}, u32[]{:S(2)}) collective-permute-start(bf16[2048,256]{1,0:T(8,128)(2,1)} %collective-permute-done.4), channel_id=1, source_target_pairs={{0,2},{1,3},{2,0},{3,1},{4,6},{5,7},{6,4},{7,5},{8,10},{9,11},{10,... | collective-permute-start | bytes 3145736 | tf_op jit(solution)/shard_map/ppermute | solution.py:111
  69.9 12.5 %collective-permute-start.9 = (bf16[128,2048]{1,0:T(8,128)(2,1)}, bf16[128,2048]{1,0:T(8,128)(2,1)}, u32[]{:S(2)}, u32[]{:S(2)}) collective-permute-start(bf16[128,2048]{1,0:T(8,128)(2,1)} %collective-permute-done.8), channel_id=1, source_target_pairs={{0,2},{1,3},{2,0},{3,1},{4,6},{5,7},{6,4},{7,5},{8,10},{9,11},{10,... | collective-permute-start | bytes 1572872 | tf_op jit(solution)/shard_map/ppermute | solution.py:111
  70.4 14.2 %collective-permute-start.6 = (bf16[2048,256]{1,0:T(8,128)(2,1)}, bf16[2048,256]{1,0:T(8,128)(2,1)S(1)}, u32[]{:S(2)}, u32[]{:S(2)}) collective-permute-start(bf16[2048,256]{1,0:T(8,128)(2,1)} %collective-permute-done.4), channel_id=1, source_target_pairs={{0,1},{1,0},{2,3},{3,2},{4,5},{5,4},{6,7},{7,6},{8,9},{9,8},{10,11... | collective-permute-start | bytes 3145736 | tf_op jit(solution)/shard_map/ppermute | solution.py:111
  75.0 31.5 %collective-permute-start.10 = (bf16[128,2048]{1,0:T(8,128)(2,1)}, bf16[128,2048]{1,0:T(8,128)(2,1)}, u32[]{:S(2)}, u32[]{:S(2)}) collective-permute-start(bf16[128,2048]{1,0:T(8,128)(2,1)} %collective-permute-done.8), channel_id=1, source_target_pairs={{0,1},{1,0},{2,3},{3,2},{4,5},{5,4},{6,7},{7,6},{8,9},{9,8},{10,11... | collective-permute-start | bytes 1572872 | tf_op jit(solution)/shard_map/ppermute | solution.py:111
  75.5 10.2 %collective-permute-start.7 = (bf16[2048,256]{1,0:T(8,128)(2,1)}, bf16[2048,256]{1,0:T(8,128)(2,1)S(1)}, u32[]{:S(2)}, u32[]{:S(2)}) collective-permute-start(bf16[2048,256]{1,0:T(8,128)(2,1)} %collective-permute-done.5), channel_id=1, source_target_pairs={{0,1},{1,0},{2,3},{3,2},{4,5},{5,4},{6,7},{7,6},{8,9},{9,8},{10,11... | collective-permute-start | bytes 3145736 | tf_op jit(solution)/shard_map/ppermute | solution.py:111
  82.4 24.1 %collective-permute-start.11 = (bf16[128,2048]{1,0:T(8,128)(2,1)}, bf16[128,2048]{1,0:T(8,128)(2,1)}, u32[]{:S(2)}, u32[]{:S(2)}) collective-permute-start(bf16[128,2048]{1,0:T(8,128)(2,1)} %collective-permute-done.9), channel_id=1, source_target_pairs={{0,1},{1,0},{2,3},{3,2},{4,5},{5,4},{6,7},{7,6},{8,9},{9,8},{10,11... | collective-permute-start | bytes 1572872 | tf_op jit(solution)/shard_map/ppermute | solution.py:111
  99.7 3.6 %copy-start.3 = (bf16[2048,128]{1,0:T(8,128)(2,1)S(1)}, bf16[2048,128]{1,0:T(8,128)(2,1)}, u32[]{:S(2)}) copy-start(bf16[2048,128]{1,0:T(8,128)(2,1)} %get-tuple-element.30) | copy-start | bytes 1572868
  99.7 3.6 %copy-start.4 = (bf16[2048,128]{1,0:T(8,128)(2,1)S(1)}, bf16[2048,128]{1,0:T(8,128)(2,1)}, u32[]{:S(2)}) copy-start(bf16[2048,128]{1,0:T(8,128)(2,1)} %get-tuple-element.32) | copy-start | bytes 1572868
  99.7 3.6 %copy-start.5 = (bf16[2048,128]{1,0:T(8,128)(2,1)S(1)}, bf16[2048,128]{1,0:T(8,128)(2,1)}, u32[]{:S(2)}) copy-start(bf16[2048,128]{1,0:T(8,128)(2,1)} %get-tuple-element.34) | copy-start | bytes 1572868
  103.3 3.2 %copy-start.7 = (bf16[576,2048]{1,0:T(8,128)(2,1)S(1)}, bf16[576,2048]{1,0:T(8,128)(2,1)}, u32[]{:S(2)}) copy-start(bf16[576,2048]{1,0:T(8,128)(2,1)} %convolution_convert_fusion.3) | copy-start | bytes 7077892
  111.1 59.4 %all-to-all-start.1 = ((bf16[4,144,2048]{2,1,0:T(8,128)(2,1)}), bf16[4,144,2048]{2,1,0:T(8,128)(2,1)}, u32[]{:S(2)}, u32[]{:S(2)}) async-start(bf16[4,144,2048]{2,1,0:T(8,128)(2,1)} %bitcast.59), calls=%async_computation.1 | async-start | bytes 4718592 | tf_op jit(solution)/shard_map/all_to_all | solution.py:200
  118.2 25.1 %collective-permute-start.1 = (bf16[256,2048]{1,0:T(8,128)(2,1)S(1)}, bf16[256,2048]{1,0:T(8,128)(2,1)S(1)}, u32[]{:S(2)}, u32[]{:S(2)}) collective-permute-start(bf16[256,2048]{1,0:T(8,128)(2,1)S(1)} %get-tuple-element.24), channel_id=1, source_target_pairs={{0,3},{1,2},{2,1},{3,0},{4,7},{5,6},{6,5},{7,4},{8,11},{9,10},{10,... | collective-permute-start | bytes 3145736 | tf_op jit(solution)/shard_map/ppermute | solution.py:111
  119.6 46.6 %collective-permute-start.2 = (bf16[256,2048]{1,0:T(8,128)(2,1)S(1)}, bf16[256,2048]{1,0:T(8,128)(2,1)S(1)}, u32[]{:S(2)}, u32[]{:S(2)}) collective-permute-start(bf16[256,2048]{1,0:T(8,128)(2,1)S(1)} %get-tuple-element.26), channel_id=1, source_target_pairs={{0,2},{1,3},{2,0},{3,1},{4,6},{5,7},{6,4},{7,5},{8,10},{9,11},{10,... | collective-permute-start | bytes 3145736 | tf_op jit(solution)/shard_map/ppermute | solution.py:111
  120.1 46.0 %collective-permute-start.3 = (bf16[256,2048]{1,0:T(8,128)(2,1)S(1)}, bf16[256,2048]{1,0:T(8,128)(2,1)S(1)}, u32[]{:S(2)}, u32[]{:S(2)}) collective-permute-start(bf16[256,2048]{1,0:T(8,128)(2,1)S(1)} %get-tuple-element.25), channel_id=1, source_target_pairs={{0,1},{1,0},{2,3},{3,2},{4,5},{5,4},{6,7},{7,6},{8,9},{9,8},{10,11... | collective-permute-start | bytes 3145736 | tf_op jit(solution)/shard_map/ppermute | solution.py:111
